TPU v7x, 32 devices: a whole 2x2x4 slice. The times are simulated.
32 devices in a mesh: sp: 4 (over z), dp: 8 (over y, x, core).
Axes of the slice: x: 2, y: 2, z: 4, core: 2. Of those that a mesh axis runs over, the one named last changes fastest.
Arguments:
- query_rows: bfloat16 [8, 512, 1024], P('dp', 'sp'), may hold values from -5.5 to 5.5
- key_rows: bfloat16 [8, 512, 1024], P('dp', 'sp'), may hold values from -5.5 to 5.5
- value_rows: bfloat16 [8, 512, 1024], P('dp', 'sp'), may hold values from -6 to 6
- lambdas: float32 [8], replicated, may hold values from 0.3 to 0.8
- query_gain: float32 [64], replicated, may hold values from 1.1 to 8
- key_gain: float32 [64], replicated, may hold values from 1.1 to 8
- sub_gain: float32 [128], replicated, may hold values from 0.1 to 1.9
- out_weight: bfloat16 [1024, 2048], P(None, 'dp'), may hold values from -0.1875 to 0.1875
Outputs:
- attended: bfloat16 [8, 512, 2048], P('dp', 'sp')
All inputs are finite; a program needn't handle non-finite values.
Results may differ from a plain program's by a relative error of at most 0.0025.
The roundings to bfloat16 on the way count: a program that leaves them out, or rounds other values in their place, can miss the bound.
Values may be sent and summed in bfloat16 or wider, within the bound.
A program may use at most 64 MiB of HBM per device.

v0:
```python
import jax
import jax.numpy as jnp
from jax import lax
from jax.sharding import PartitionSpec as P

D = 2048
HEADS = 8
HK = 64
HV = 128


epsilon = 1e-06
output_scale = 0.8


def normalize(field, scaling):
    return field * lax.rsqrt(jnp.mean(field * field, axis=-1, keepdims=True) + epsilon) * scaling


def attend(arrived, length):
    block_rows = max(min(512, length), length // 16)
    results = []
    for number in range(length // block_rows):
        first_row = number * block_rows
        last_row = first_row + block_rows
        query_block = arrived[first_row:last_row, :, :HK]
        key_block = arrived[:last_row, :, HK : 2 * HK]
        value_block = arrived[:last_row, :, 2 * HK :]
        scores = jnp.einsum(
            "qgd,kgd->gqk", query_block, key_block, preferred_element_type=jnp.float32
        ) * HK ** (-0.5)
        visible = jnp.arange(last_row)[None, :] <= (first_row + jnp.arange(block_rows))[:, None]
        scores = jnp.where(visible[None], scores, -jnp.inf)
        weights = jax.nn.softmax(scores, axis=-1).astype(jnp.bfloat16)
        results.append(
            jnp.einsum(
                "gqk,kgd->qgd", weights, value_block, preferred_element_type=jnp.float32
            ).astype(jnp.bfloat16)
        )
    return jnp.concatenate(results, axis=0)


def body(query_rows, key_rows, value_rows, lambdas, query_gain, key_gain, sub_gain, out_weight):
    sequences = query_rows.shape[0]
    tokens_here = query_rows.shape[1]
    groups = 2 * HEADS
    query_norm = normalize(
        query_rows.reshape(sequences, tokens_here, groups, HK).astype(jnp.float32), query_gain
    ).astype(jnp.bfloat16)
    key_norm = normalize(
        key_rows.reshape(sequences, tokens_here, groups, HK).astype(jnp.float32), key_gain
    ).astype(jnp.bfloat16)
    value_heads = value_rows.reshape(sequences, tokens_here, HEADS, HV)
    packet = jnp.concatenate(
        [query_norm, key_norm, jnp.concatenate([value_heads, value_heads], axis=2)], axis=3
    )
    arrived = lax.all_to_all(packet, "sp", split_axis=2, concat_axis=1, tiled=True)
    length = arrived.shape[1]
    map_outputs = attend(arrived[0], length)[None]
    returned = lax.all_to_all(map_outputs, "sp", split_axis=1, concat_axis=2, tiled=True)
    returned_float = returned.astype(jnp.float32)
    mixed_heads = returned_float[:, :, :HEADS] - lambdas[:, None] * returned_float[:, :, HEADS:]
    normed = (
        (normalize(mixed_heads, sub_gain) * output_scale)
        .astype(jnp.bfloat16)
        .reshape(sequences * tokens_here, HEADS * HV)
    )
    projected = jnp.dot(
        normed,
        lax.all_gather(out_weight, "dp", axis=1, tiled=True),
        preferred_element_type=jnp.float32,
    )
    return projected.astype(jnp.bfloat16).reshape(sequences, tokens_here, D)


def solution(mesh):
    in_specs = (
        P("dp", "sp", None),
        P("dp", "sp", None),
        P("dp", "sp", None),
        P(),
        P(),
        P(),
        P(),
        P(None, "dp"),
    )
    out_specs = P("dp", "sp", None)
    return jax.shard_map(body, mesh=mesh, in_specs=in_specs, out_specs=out_specs, check_vma=False)
```

profile of v0, /device:TPU:0, one launch (start us, length us, event | category | flops | bytes accessed | tf_op | source)
XLA Modules:
  0.0 81.3 jit_solution(6147966888344264109)
XLA Ops:
  6.5 0.0 all-gather.2.cloned.1.call-start
  6.5 0.7 all-gather.2.cloned.1.call-update
  7.3 1.1 %copy.35 = bf16[1,128,1024]{1,2,0:T(8,128)(2,1)S(1)} copy(bf16[1,128,1024]{2,1,0:T(8,128)(2,1)} %param.9) | data formatting | bytes 524288 | tf_op args[1]
  8.4 1.1 %copy.34 = bf16[1,128,1024]{1,2,0:T(8,128)(2,1)S(1)} copy(bf16[1,128,1024]{2,1,0:T(8,128)(2,1)} %param.8) | data formatting | bytes 524288 | tf_op args[0]
  9.5 1.1 %copy.36 = bf16[1,128,1024]{1,2,0:T(8,128)(2,1)S(1)} copy(bf16[1,128,1024]{2,1,0:T(8,128)(2,1)} %param.10) | data formatting | bytes 524288 | tf_op args[2]
  10.6 0.1 fusion.12
  10.7 0.1 fusion.9
  10.8 0.9 %fusion.11 = (bf16[1,128,16,64]{1,3,2,0:T(8,128)(2,1)S(1)}, bf16[1,128,16,64]{1,3,2,0:T(8,128)(2,1)S(1)}) fusion(f32[64]{0:T(128)} %param.12, f32[128,16]{0,1:T(8,128)S(1)} %add_rsqrt_fusion.1, bf16[1,128,1024]{1,2,0:T(8,128)(2,1)S(1)} %copy.34, f32[64]{0:T(128)} %param.13, f32[128,16]{0,1:T(8,128)S(1)} %add_rsqrt_fusion, bf16[1,128,1024]{1,2,0:T(8,128)(2,1)S(1)} %copy.35), kind=kLoop, calls=%fused_computation.22 | loop fusion | flops 1048576 | bytes 1065472 | tf_op jit(solution)/shard_map/convert_element_type | solution.py:49
  11.7 1.1 %maximum_bitcast_fusion = bf16[1,128,16,256]{1,3,0,2:T(8,128)(2,1)} fusion(bf16[1,128,8,128]{1,3,2,0:T(8,128)(2,1)S(1)} %bitcast.34, bf16[1,128,16,64]{1,3,2,0:T(8,128)(2,1)S(1)} %get-tuple-element.8, bf16[1,128,16,64]{1,3,2,0:T(8,128)(2,1)S(1)} %get-tuple-element.7), kind=kLoop, calls=%fused_computation.13 | loop fusion | flops 4194304 | bytes 1835008 | tf_op jit(solution)/shard_map/concatenate | solution.py:54
  12.8 6.3 %all-to-all-start = ((bf16[1,128,16,256]{1,3,0,2:T(8,128)(2,1)}), bf16[1,128,16,256]{1,3,0,2:T(8,128)(2,1)S(1)}, u32[]{:S(2)}, u32[]{:S(2)}) async-start(bf16[1,128,16,256]{1,3,0,2:T(8,128)(2,1)} %maximum_bitcast_fusion), calls=%async_computation | async-start | bytes 2097152 | tf_op jit(solution)/shard_map/all_to_all | solution.py:57
  19.2 0.1 iota_compare_fusion
  19.3 25.6 %all-to-all-done = bf16[1,128,16,256]{1,3,0,2:T(8,128)(2,1)S(1)} async-done(((bf16[1,128,16,256]{1,3,0,2:T(8,128)(2,1)}), bf16[1,128,16,256]{1,3,0,2:T(8,128)(2,1)S(1)}, u32[]{:S(2)}, u32[]{:S(2)}) %all-to-all-start) | async-done | bytes 1048608 | tf_op jit(solution)/shard_map/all_to_all | solution.py:57
  44.9 0.5 copy.38
  45.4 0.7 copy.39
  46.1 0.4 squeeze.3
  46.6 3.6 %fusion.32 = (f32[4,512]{1,0:T(4,128)S(1)}, f32[4,512,512]{1,2,0:T(8,128)}) fusion(pred[512,512]{0,1:T(8,128)(4,1)S(1)} %iota_compare_fusion, bf16[512,4,256]{0,2,1:T(8,128)(2,1)S(1)} %squeeze.3), kind=kOutput, calls=%fused_computation.42 | convolution fusion | flops 138412544 | bytes 4988928 | tf_op jit(solution)/shard_map/sub | solution.py:34
  50.2 2.6 %fusion.8 = bf16[1,512,4,128]{1,3,2,0:T(8,128)(2,1)S(1)} fusion(f32[4,512,512]{1,2,0:T(8,128)} %get-tuple-element.6, f32[4,512]{1,0:T(4,128)S(1)} %get-tuple-element.5, bf16[512,4,256]{0,2,1:T(8,128)(2,1)S(1)} %squeeze.3), kind=kOutput, calls=%fused_computation.12 | convolution fusion | flops 270794752 | bytes 5251072 | tf_op jit(solution)/shard_map/gqk,kgd->qgd/dot_general | solution.py:36
  52.9 0.0 copy-start
  52.9 0.0 copy-start.1
  52.9 0.3 copy.41
  53.2 16.4 %all_to_all.24 = bf16[1,512,4,128]{3,2,0,1:T(4,128)(2,1)S(1)} all-to-all(bf16[1,512,4,128]{3,2,0,1:T(4,128)(2,1)S(1)} %copy.41), channel_id=1, replica_groups=mesh['sp'=4,'dp'=8] {'sp'}, dimensions={1} | all-to-all | bytes 1048576 | tf_op jit(solution)/shard_map/all_to_all | solution.py:60
  69.7 0.1 copy.42
  69.7 0.1 convert_bitcast_fusion
  69.8 0.1 copy.43
  69.9 0.0 copy-done
  69.9 0.3 multiply_reduce_fusion
  70.2 0.0 copy-done.1
  70.2 0.3 multiply_convert_fusion
  70.5 0.2 copy.44
  70.7 0.0 all-gather.2.cloned.1.call-done
  70.7 3.7 %fusion.2 = bf16[1,128,2048]{2,1,0:T(8,128)(2,1)} fusion(bf16[128,1024]{0,1:T(8,128)(2,1)S(1)} %bitcast.35, bf16[1024,2048]{1,0:T(8,128)(2,1)} %all-gather.2.cloned.1.call-done), kind=kOutput, calls=%fused_computation.6 | convolution fusion | flops 537133056 | bytes 4980736 | tf_op jit(solution)/shard_map/dot_general | solution.py:68
  (3 shorter events, 0.0 us)
Async XLA Ops:
  6.5 64.2 %all-gather.2.cloned.1.call-start = ((), (), s32[]{:S(2)}) async-start(), calls=%async_computation.2 | async-start | bytes 4718592 | tf_op jit(solution)/shard_map/all_gather | solution.py:70
  12.8 32.1 %all-to-all-start = ((bf16[1,128,16,256]{1,3,0,2:T(8,128)(2,1)}), bf16[1,128,16,256]{1,3,0,2:T(8,128)(2,1)S(1)}, u32[]{:S(2)}, u32[]{:S(2)}) async-start(bf16[1,128,16,256]{1,3,0,2:T(8,128)(2,1)} %maximum_bitcast_fusion), calls=%async_computation | async-start | bytes 2097152 | tf_op jit(solution)/shard_map/all_to_all | solution.py:57
  52.9 17.1 %copy-start = (f32[8]{0:T(128)S(1)}, f32[8]{0:T(128)}, u32[]{:S(2)}) copy-start(f32[8]{0:T(128)} %param.11) | copy-start | bytes 100
  52.9 17.4 %copy-start.1 = (f32[128]{0:T(128)S(1)}, f32[128]{0:T(128)}, u32[]{:S(2)}) copy-start(f32[128]{0:T(128)} %param.14) | copy-start | bytes 1540
Sparse Core Ops, SparseCore 0:
  9.2 40.0 all-gather.1
where the time goes:
time: 81.7 us; the launch traced here: 81.3 us
  waiting for transfers between devices  26.4 us (32%)
  blocking collectives  16.4 us (20%)
  between operations  13.6 us (17%)
  matrix products  10 us (12%)
  starting transfers between devices  6.35 us (8%)
  local copies, waits for them, and re-layouts  5.66 us (7%)
  other arithmetic  2.87 us (4%)
    all_to_all x1, waiting for transfers between devices, body(): lax.all_to_all(packet, 'sp', split_axis=2, concat_axis=1, tiled=True)  25.6 us
    all_to_all x1, blocking collectives, body(): lax.all_to_all(map_outputs, 'sp', split_axis=1, concat_axis=2, tiled=True)  16.4 us
    all_to_all x1, starting transfers between devices, body(): lax.all_to_all(packet, 'sp', split_axis=2, concat_axis=1, tiled=True)  6.35 us
    dot_general x1, matrix products, body(): jnp.dot(normed, lax.all_gather(out_weight, 'dp', axis=1, tiled=True), pre...  3.73 us
    sub x1, matrix products, attend(): weights = jax.nn.softmax(scores, axis=-1).astype(jnp.bfloat16)  3.65 us
    unnamed x7, local copies, waits for them, and re-layouts  3.37 us
    dot_general x1, matrix products, attend(): jnp.einsum('gqk,kgd->qgd', weights, value_block, preferred_element_type=j...  2.64 us
  transfers between devices with their start and end apart: 2, of which 1 were waited for; matrix products, arithmetic and copies ran while one was open for 18% of the time, Pallas kernels for 0%

commit v1 on v0

--- a/solution.py
+++ b/solution.py
@@ -1,6 +1,10 @@
+import functools
+
 import jax
 import jax.numpy as jnp
 from jax import lax
+from jax.experimental import pallas as pl
+from jax.experimental.pallas import tpu as pltpu
 from jax.sharding import PartitionSpec as P
 
 D = 2048
@@ -73,6 +77,247 @@
     return projected.astype(jnp.bfloat16).reshape(sequences, tokens_here, D)
 
 
+MESH = pl.DeviceIdType.MESH
+
+
+def fits(sp, dp, rows_shape, weight_shape):
+    if HEADS % sp or (HEADS // sp * HK) % 128 or dp % 2:
+        return False
+    return rows_shape[0] == 1 and rows_shape[1] % 128 == 0 and rows_shape[1] * sp <= 1024 and weight_shape[1] % 128 == 0
+
+
+def kernel(
+    sp, dp, q_ref, k_ref, v_ref, lam_ref, qg_ref, kg_ref, sg_ref, w_ref, out_ref,
+    qb, kb, vb, kn, first, nsend, nbuf, wbuf,
+    in_send, in_recv, back_send, back_recv, w_send, w_recv, p_send, p_recv,
+):
+    me, d = lax.axis_index("sp"), lax.axis_index("dp")
+    partner = d + 1 - 2 * lax.rem(d, 2)
+    chips = dp // 2
+    rows = q_ref.shape[0]
+    local = HEADS // sp
+    width, vwidth = local * HK, local * HV
+    columns = w_ref.shape[1]
+
+    barrier = pltpu.get_barrier_semaphore()
+    for o in range(1, sp):
+        pl.semaphore_signal(barrier, inc=1, device_id=(lax.rem(me + o, sp), d), device_id_type=MESH)
+    for c in range(1, chips):
+        pl.semaphore_signal(barrier, inc=1, device_id=(me, lax.rem(d + 2 * c, dp)), device_id_type=MESH)
+    pl.semaphore_signal(barrier, inc=1, device_id=(me, partner), device_id_type=MESH)
+    pl.semaphore_wait(barrier, sp - 1 + chips)
+
+    def span(i):
+        return pl.ds(pl.multiple_of(i * rows, rows), rows)
+
+    def pieces(target, source):
+        low = pl.ds(pl.multiple_of(target * width, 128), width)
+        high = pl.ds(pl.multiple_of(HEADS * HK + target * width, 128), width)
+        vals = pl.ds(pl.multiple_of(target * vwidth, 128), vwidth)
+        there = span(source)
+        return (
+            (k_ref.at[:, low], kb.at[0, there, :]),
+            (q_ref.at[:, low], qb.at[0, there, :]),
+            (v_ref.at[:, vals], vb.at[there, :]),
+            (k_ref.at[:, high], kb.at[1, there, :]),
+            (q_ref.at[:, high], qb.at[1, there, :]),
+        )
+
+    def forward(o, t):
+        target = lax.rem(me + o, sp)
+        src, dst = pieces(target, me)[t]
+        return pltpu.make_async_remote_copy(
+            src_ref=src, dst_ref=dst, send_sem=in_send.at[o, t], recv_sem=in_recv.at[me, t],
+            device_id=(target, d), device_id_type=MESH,
+        )
+
+    def mine(t):
+        src, dst = pieces(me, me)[t]
+        return pltpu.make_async_copy(src, dst, in_recv.at[me, t])
+
+    def arrived(i, t):
+        @pl.when(i == me)
+        def _():
+            mine(t).wait()
+
+        @pl.when(i != me)
+        def _():
+            src, dst = pieces(me, i)[t]
+            pltpu.make_async_remote_copy(
+                src_ref=src, dst_ref=dst, send_sem=in_send.at[0, t], recv_sem=in_recv.at[i, t],
+                device_id=(me, d), device_id_type=MESH,
+            ).wait_recv()
+
+    def spread(c):
+        return pltpu.make_async_remote_copy(
+            src_ref=w_ref, dst_ref=wbuf.at[d], send_sem=w_send.at[c], recv_sem=w_recv.at[c],
+            device_id=(me, lax.rem(d + 2 * c, dp)), device_id_type=MESH,
+        )
+
+    def shard_of(device, c):
+        return lax.rem(device - 2 * c + dp, dp)
+
+    def pair(c):
+        at = shard_of(d, c)
+        return pltpu.make_async_remote_copy(
+            src_ref=w_ref if c == 0 else wbuf.at[at], dst_ref=wbuf.at[at],
+            send_sem=p_send.at[c], recv_sem=p_recv.at[c],
+            device_id=(me, partner), device_id_type=MESH,
+        )
+
+    def back(i):
+        return pltpu.make_async_remote_copy(
+            src_ref=nsend.at[i], dst_ref=nbuf.at[me], send_sem=back_send.at[i], recv_sem=back_recv.at[me],
+            device_id=(i, d), device_id_type=MESH,
+        )
+
+    for t in range(5):
+        mine(t).start()
+        for o in range(1, sp):
+            forward(o, t).start()
+        if t == 0:
+            for c in range(1, chips):
+                spread(c).start()
+            pair(0).start()
+
+    lane = lax.broadcasted_iota(jnp.int32, (width, width), 1) // HK
+    ones = (lane == lax.broadcasted_iota(jnp.int32, (width, width), 0) // HK).astype(jnp.bfloat16)
+    head_of = lax.broadcasted_iota(jnp.int32, (rows, width), 1) // HK
+    visible = lax.broadcasted_iota(jnp.int32, (rows, rows), 1) <= lax.broadcasted_iota(jnp.int32, (rows, rows), 0)
+    visible = jnp.concatenate([visible] * local, axis=0)
+    query_gain = jnp.concatenate([qg_ref[...]] * local, axis=1)
+    key_gain = jnp.concatenate([kg_ref[...]] * local, axis=1)
+    sub_gain = sg_ref[...] * output_scale
+
+    def normed_rows(block, gain):
+        field = block.astype(jnp.float32)
+        square = field * field
+        upper = square.astype(jnp.bfloat16)
+        lower = (square - upper.astype(jnp.float32)).astype(jnp.bfloat16)
+        total = jnp.dot(upper, ones, preferred_element_type=jnp.float32)
+        total += jnp.dot(lower, ones, preferred_element_type=jnp.float32)
+        return (field * lax.rsqrt(total * (1.0 / HK) + epsilon) * gain).astype(jnp.bfloat16)
+
+    def attend_block(m, i):
+        base, keys = i * rows, (i + 1) * rows
+        kn[m, base:keys, :] = normed_rows(kb[m, base:keys, :], key_gain)
+        query = normed_rows(qb[m, base:keys, :], query_gain)
+        zero = jnp.zeros_like(query)
+        stacked = jnp.concatenate([jnp.where(head_of == h, query, zero) for h in range(local)], axis=0)
+        scores = lax.dot_general(
+            stacked, kn[m, :keys, :], (((1,), (1,)), ((), ())), preferred_element_type=jnp.float32
+        ) * HK ** (-0.5)
+        last = jnp.where(visible, scores[:, base:], -jnp.inf)
+        scores = last if i == 0 else jnp.concatenate([scores[:, :base], last], axis=1)
+        raised = jnp.exp(scores - jnp.max(scores, axis=1, keepdims=True))
+        weights = (raised * (1.0 / jnp.sum(raised, axis=1, keepdims=True))).astype(jnp.bfloat16)
+        return [
+            jnp.dot(
+                weights[h * rows : (h + 1) * rows], vb[:keys, h * HV : (h + 1) * HV],
+                preferred_element_type=jnp.float32,
+            ).astype(jnp.bfloat16)
+            for h in range(local)
+        ]
+
+    for i in range(sp):
+        for t in range(3):
+            arrived(i, t)
+        for h, part in enumerate(attend_block(0, i)):
+            first[i * rows : (i + 1) * rows, h * HV : (h + 1) * HV] = part
+
+    for i in range(sp):
+        for t in range(3, 5):
+            arrived(i, t)
+        for h, part in enumerate(attend_block(1, i)):
+            before = first[i * rows : (i + 1) * rows, h * HV : (h + 1) * HV].astype(jnp.float32)
+            mixed = before - lam_ref[me * local + h] * part.astype(jnp.float32)
+            mean = jnp.mean(mixed * mixed, axis=1, keepdims=True)
+            nsend[i, :, h * HV : (h + 1) * HV] = (mixed * lax.rsqrt(mean + epsilon) * sub_gain).astype(jnp.bfloat16)
+
+        @pl.when(i == me)
+        def _():
+            nbuf[i] = nsend[i]
+
+        @pl.when(i != me)
+        def _():
+            back(i).start()
+
+    for c in range(1, chips):
+        spread(c).wait_recv()
+        pair(c).start()
+
+    for i in range(sp):
+        @pl.when(i != me)
+        def _():
+            pltpu.make_async_remote_copy(
+                src_ref=nsend.at[i], dst_ref=nbuf.at[i], send_sem=back_send.at[i], recv_sem=back_recv.at[i],
+                device_id=(i, d), device_id_type=MESH,
+            ).wait_recv()
+
+    normed = jnp.concatenate([nbuf[j] for j in range(sp)], axis=1)
+
+    def project(shard, weight):
+        out_ref[:, pl.ds(pl.multiple_of(shard * columns, 128), columns)] = jnp.dot(
+            normed, weight, preferred_element_type=jnp.float32
+        ).astype(jnp.bfloat16)
+
+    project(d, w_ref[...])
+    for c in range(1, chips):
+        project(shard_of(d, c), wbuf[shard_of(d, c)])
+    for c in range(chips):
+        at = shard_of(partner, c)
+        pltpu.make_async_remote_copy(
+            src_ref=w_ref, dst_ref=wbuf.at[at], send_sem=p_send.at[c], recv_sem=p_recv.at[c],
+            device_id=(me, partner), device_id_type=MESH,
+        ).wait_recv()
+        project(at, wbuf[at])
+
+    for o in range(1, sp):
+        for t in range(5):
+            forward(o, t).wait_send()
+    for c in range(chips):
+        pair(c).wait_send()
+        if c:
+            spread(c).wait_send()
+    for i in range(sp):
+        @pl.when(i != me)
+        def _():
+            back(i).wait_send()
+
+
+def fused(sp, dp, query_rows, key_rows, value_rows, lambdas, query_gain, key_gain, sub_gain, out_weight):
+    rows = query_rows.shape[1]
+    length = rows * sp
+    local = HEADS // sp
+    width, vwidth = local * HK, local * HV
+    depth, columns = out_weight.shape
+    vmem = pl.BlockSpec(memory_space=pltpu.VMEM)
+    dma = pltpu.SemaphoreType.DMA
+    out = pl.pallas_call(
+        functools.partial(kernel, sp, dp),
+        out_shape=jax.ShapeDtypeStruct((rows, columns * dp), jnp.bfloat16),
+        in_specs=[vmem] * 3 + [pl.BlockSpec(memory_space=pltpu.SMEM)] + [vmem] * 4,
+        out_specs=vmem,
+        scratch_shapes=[
+            pltpu.VMEM((2, length, width), jnp.bfloat16),
+            pltpu.VMEM((2, length, width), jnp.bfloat16),
+            pltpu.VMEM((length, vwidth), jnp.bfloat16),
+            pltpu.VMEM((2, length, width), jnp.bfloat16),
+            pltpu.VMEM((length, vwidth), jnp.bfloat16),
+            pltpu.VMEM((sp, rows, vwidth), jnp.bfloat16),
+            pltpu.VMEM((sp, rows, vwidth), jnp.bfloat16),
+            pltpu.VMEM((dp, depth, columns), jnp.bfloat16),
+            dma((sp, 5)), dma((sp, 5)), dma((sp,)), dma((sp,)),
+            dma((dp // 2,)), dma((dp // 2,)), dma((dp // 2,)), dma((dp // 2,)),
+        ],
+        compiler_params=pltpu.CompilerParams(collective_id=0, has_side_effects=True),
+    )(
+        query_rows[0], key_rows[0], value_rows[0], lambdas,
+        query_gain[None], key_gain[None], sub_gain[None], out_weight,
+    )
+    return out[None]
+
+
 def solution(mesh):
     in_specs = (
         P("dp", "sp", None),
@@ -85,4 +330,11 @@
         P(None, "dp"),
     )
     out_specs = P("dp", "sp", None)
-    return jax.shard_map(body, mesh=mesh, in_specs=in_specs, out_specs=out_specs, check_vma=False)
+    sp, dp = mesh.shape["sp"], mesh.shape["dp"]
+
+    def step(*operands):
+        if fits(sp, dp, operands[0].shape, operands[7].shape):
+            return fused(sp, dp, *operands)
+        return body(*operands)
+
+    return jax.shard_map(step, mesh=mesh, in_specs=in_specs, out_specs=out_specs, check_vma=False)

time: 81.7 us -> 36.8 us (0.45)
  Pallas kernels: 0 us -> 34.5 us
  waiting for transfers between devices: 26.4 us -> 0 us
  blocking collectives: 16.4 us -> 0 us
  between operations: 13.6 us -> 0.01 us
  matrix products: 10 us -> 0 us
  starting transfers between devices: 6.35 us -> 0 us
  local copies, waits for them, and re-layouts: 5.66 us -> 1.88 us
  other arithmetic: 2.87 us -> 0 us
    pallas_call x0 -> x1, Pallas kernels: none -> 34.5 us  [fused(): pl.pallas_call(functools.partial(kernel, sp, dp), out_shape=jax.ShapeDtyp...]
    all_to_all x1 -> x0, waiting for transfers between devices: 25.6 us -> none  [body(): lax.all_to_all(packet, 'sp', split_axis=2, concat_axis=1, tiled=True)]
    all_to_all x1 -> x0, blocking collectives: 16.4 us -> none  [body(): lax.all_to_all(map_outputs, 'sp', split_axis=1, concat_axis=2, tiled=True)]
    dot_general x2 -> x0, matrix products: 6.37 us -> none  [the longest x1 3.73 us: body(): jnp.dot(normed, lax.all_gather(out_weight, 'dp', axis=1, tiled=True), pre...]
    all_to_all x1 -> x0, starting transfers between devices: 6.35 us -> none  [body(): lax.all_to_all(packet, 'sp', split_axis=2, concat_axis=1, tiled=True)]
    sub x1 -> x0, matrix products: 3.65 us -> none  [attend(): weights = jax.nn.softmax(scores, axis=-1).astype(jnp.bfloat16)]
    unnamed x7 -> x1, local copies, waits for them, and re-layouts: 3.37 us -> 1.88 us
    all_to_all x3 -> x0, local copies, waits for them, and re-layouts: 1.27 us -> none  [the longest x2 1.2 us: body(): lax.all_to_all(packet, 'sp', split_axis=2, concat_axis=1, tiled=True)]
  transfers between devices with their start and end apart: 2 -> 0, of which waited for: 1 -> 0; matrix products, arithmetic and copies ran while one was open for 18% -> 0% of each run, Pallas kernels for 0% -> 0%
where the time goes in v1:
time: 36.8 us; the launch traced here: 36.4 us
  Pallas kernels  34.5 us (94%)
  local copies, waits for them, and re-layouts  1.88 us (5%)
    pallas_call x1, Pallas kernels, fused(): pl.pallas_call(functools.partial(kernel, sp, dp), out_shape=jax.ShapeDtyp...  34.5 us
    unnamed x1, local copies, waits for them, and re-layouts  1.88 us

profile of v1, /device:TPU:0, one launch (start us, length us, event | category | flops | bytes accessed | tf_op | source)
XLA Modules:
  0.0 36.4 jit_solution(17879665011500353123)
XLA Ops:
  0.0 34.5 %shard_map.82 = bf16[128,2048]{1,0:T(8,128)(2,1)} custom-call(bf16[128,1024]{1,0:T(8,128)(2,1)} %bitcast.8, bf16[128,1024]{1,0:T(8,128)(2,1)} %bitcast.9, bf16[128,1024]{1,0:T(8,128)(2,1)} %bitcast.10, f32[8]{0:T(128)} %lam_ref.1, f32[1,64]{1,0:T(1,128)} %bitcast.11, f32[1,64]{1,0:T(1,128)} %bitcast.12, f32[1,128]{1,0:T(1,128)} %bitcast.13, ...), custom_call_target="tpu_custom_call" | custom-call | tf_op jit(solution)/shard_map/pallas_call | solution.py:296
  34.5 1.9 %copy.10 = bf16[1,128,2048]{2,1,0:T(8,128)(2,1)} copy(bf16[1,128,2048]{2,1,0:T(8,128)(2,1)} %bitcast.7) | data formatting | bytes 1048576

commit v2 on v1

--- a/solution.py
+++ b/solution.py
@@ -89,7 +89,7 @@
 def kernel(
     sp, dp, q_ref, k_ref, v_ref, lam_ref, qg_ref, kg_ref, sg_ref, w_ref, out_ref,
     qb, kb, vb, kn, first, nsend, nbuf, wbuf,
-    in_send, in_recv, back_send, back_recv, w_send, w_recv, p_send, p_recv,
+    in_send, in_recv, back_send, back_recv, w_send, w_recv, p_send, p_recv, own_sem,
 ):
     me, d = lax.axis_index("sp"), lax.axis_index("dp")
     partner = d + 1 - 2 * lax.rem(d, 2)
@@ -97,13 +97,24 @@
     rows = q_ref.shape[0]
     local = HEADS // sp
     width, vwidth = local * HK, local * HV
-    columns = w_ref.shape[1]
+    depth, columns = w_ref.shape
+    half = depth // 2
+    square = chips == 4
+
+    def fellow(c, device=d):
+        if not square:
+            return lax.rem(device + 2 * c, dp)
+        core, chip = lax.rem(device, 2), device // 2
+        x, y = lax.rem(chip, 2), chip // 2
+        x = 1 - x if c % 2 else x
+        y = 1 - y if c // 2 else y
+        return (y * 2 + x) * 2 + core
 
     barrier = pltpu.get_barrier_semaphore()
     for o in range(1, sp):
         pl.semaphore_signal(barrier, inc=1, device_id=(lax.rem(me + o, sp), d), device_id_type=MESH)
     for c in range(1, chips):
-        pl.semaphore_signal(barrier, inc=1, device_id=(me, lax.rem(d + 2 * c, dp)), device_id_type=MESH)
+        pl.semaphore_signal(barrier, inc=1, device_id=(me, fellow(c)), device_id_type=MESH)
     pl.semaphore_signal(barrier, inc=1, device_id=(me, partner), device_id_type=MESH)
     pl.semaphore_wait(barrier, sp - 1 + chips)
 
@@ -148,14 +159,33 @@
                 device_id=(me, d), device_id_type=MESH,
             ).wait_recv()
 
-    def spread(c):
+    def rows_of(h):
+        return pl.ds(h * half, half)
+
+    def spread(c, h):
+        source, over = d, c
+        if square and c == 3:
+            source, over = fellow(1 + h), 2 - h
+        src = w_ref if source is d else wbuf.at[source]
         return pltpu.make_async_remote_copy(
-            src_ref=w_ref, dst_ref=wbuf.at[d], send_sem=w_send.at[c], recv_sem=w_recv.at[c],
-            device_id=(me, lax.rem(d + 2 * c, dp)), device_id_type=MESH,
+            src_ref=src.at[rows_of(h)], dst_ref=wbuf.at[source, rows_of(h)], send_sem=w_send.at[c, h], recv_sem=w_recv.at[c, h],
+            device_id=(me, fellow(over)), device_id_type=MESH,
         )
 
     def shard_of(device, c):
-        return lax.rem(device - 2 * c + dp, dp)
+        if c == 0:
+            return device
+        return fellow(c, device) if square else lax.rem(device - 2 * c + dp, dp)
+
+    def own_weights():
+        return pltpu.make_async_copy(w_ref, wbuf.at[d], own_sem)
+
+    def gained(c, h):
+        at = shard_of(d, c)
+        pltpu.make_async_remote_copy(
+            src_ref=wbuf.at[at, rows_of(h)], dst_ref=wbuf.at[at, rows_of(h)], send_sem=w_send.at[c, h], recv_sem=w_recv.at[c, h],
+            device_id=(me, partner), device_id_type=MESH,
+        ).wait_recv()
 
     def pair(c):
         at = shard_of(d, c)
@@ -176,9 +206,16 @@
         for o in range(1, sp):
             forward(o, t).start()
         if t == 0:
-            for c in range(1, chips):
-                spread(c).start()
+            for order in range(2):
+                for c in range(1, chips):
+                    if not (square and c == 3):
+                        spread(c, (c + 1 + order) % 2).start()
             pair(0).start()
+            own_weights().start()
+    if square:
+        for h in range(2):
+            gained(1 + h, h)
+            spread(3, h).start()
 
     lane = lax.broadcasted_iota(jnp.int32, (width, width), 1) // HK
     ones = (lane == lax.broadcasted_iota(jnp.int32, (width, width), 0) // HK).astype(jnp.bfloat16)
@@ -225,6 +262,11 @@
         for h, part in enumerate(attend_block(0, i)):
             first[i * rows : (i + 1) * rows, h * HV : (h + 1) * HV] = part
 
+    if square:
+        for h in range(2):
+            gained(1 + h, 1 - h)
+            pair(1 + h).start()
+
     for i in range(sp):
         for t in range(3, 5):
             arrived(i, t)
@@ -242,8 +284,9 @@
         def _():
             back(i).start()
 
-    for c in range(1, chips):
-        spread(c).wait_recv()
+    for c in range(3 if square else 1, chips):
+        for h in range(2):
+            gained(c, h)
         pair(c).start()
 
     for i in range(sp):
@@ -261,13 +304,13 @@
             normed, weight, preferred_element_type=jnp.float32
         ).astype(jnp.bfloat16)
 
-    project(d, w_ref[...])
-    for c in range(1, chips):
+    own_weights().wait()
+    for c in range(chips):
         project(shard_of(d, c), wbuf[shard_of(d, c)])
     for c in range(chips):
         at = shard_of(partner, c)
         pltpu.make_async_remote_copy(
-            src_ref=w_ref, dst_ref=wbuf.at[at], send_sem=p_send.at[c], recv_sem=p_recv.at[c],
+            src_ref=wbuf.at[at], dst_ref=wbuf.at[at], send_sem=p_send.at[c], recv_sem=p_recv.at[c],
             device_id=(me, partner), device_id_type=MESH,
         ).wait_recv()
         project(at, wbuf[at])
@@ -278,7 +321,8 @@
     for c in range(chips):
         pair(c).wait_send()
         if c:
-            spread(c).wait_send()
+            for h in range(2):
+                spread(c, h).wait_send()
     for i in range(sp):
         @pl.when(i != me)
         def _():
@@ -292,11 +336,12 @@
     width, vwidth = local * HK, local * HV
     depth, columns = out_weight.shape
     vmem = pl.BlockSpec(memory_space=pltpu.VMEM)
+    hbm = pl.BlockSpec(memory_space=pl.ANY)
     dma = pltpu.SemaphoreType.DMA
     out = pl.pallas_call(
         functools.partial(kernel, sp, dp),
-        out_shape=jax.ShapeDtypeStruct((rows, columns * dp), jnp.bfloat16),
-        in_specs=[vmem] * 3 + [pl.BlockSpec(memory_space=pltpu.SMEM)] + [vmem] * 4,
+        out_shape=pltpu.VMEM((rows, columns * dp), jnp.bfloat16),
+        in_specs=[hbm] * 3 + [pl.BlockSpec(memory_space=pltpu.SMEM)] + [vmem] * 3 + [hbm],
         out_specs=vmem,
         scratch_shapes=[
             pltpu.VMEM((2, length, width), jnp.bfloat16),
@@ -308,7 +353,7 @@
             pltpu.VMEM((sp, rows, vwidth), jnp.bfloat16),
             pltpu.VMEM((dp, depth, columns), jnp.bfloat16),
             dma((sp, 5)), dma((sp, 5)), dma((sp,)), dma((sp,)),
-            dma((dp // 2,)), dma((dp // 2,)), dma((dp // 2,)), dma((dp // 2,)),
+            dma((dp // 2, 2)), dma((dp // 2, 2)), dma((dp // 2,)), dma((dp // 2,)), dma,
         ],
         compiler_params=pltpu.CompilerParams(collective_id=0, has_side_effects=True),
     )(

time: 36.8 us -> 33.1 us (0.90)
  Pallas kernels: 34.5 us -> 32.1 us
  local copies, waits for them, and re-layouts: 1.88 us -> 0.8 us
    pallas_call x1, Pallas kernels: 34.5 us -> 32.1 us  [fused(): pl.pallas_call(functools.partial(kernel, sp, dp), out_shape=pltpu.VMEM((r...]
    unnamed x1, local copies, waits for them, and re-layouts: 1.88 us -> 0.8 us
where the time goes in v2:
time: 33.1 us; the launch traced here: 32.9 us
  Pallas kernels  32.1 us (97%)
  local copies, waits for them, and re-layouts  0.8 us (2%)
    pallas_call x1, Pallas kernels, fused(): pl.pallas_call(functools.partial(kernel, sp, dp), out_shape=pltpu.VMEM((r...  32.1 us
    unnamed x1, local copies, waits for them, and re-layouts  0.8 us

profile of v2, /device:TPU:0, one launch (start us, length us, event | category | flops | bytes accessed | tf_op | source)
XLA Modules:
  0.0 32.9 jit_solution(11970834987857530728)
XLA Ops:
  0.0 32.1 %shard_map.82 = bf16[128,2048]{1,0:T(8,128)(2,1)S(1)} custom-call(bf16[128,1024]{1,0:T(8,128)(2,1)} %bitcast.8, bf16[128,1024]{1,0:T(8,128)(2,1)} %bitcast.9, bf16[128,1024]{1,0:T(8,128)(2,1)} %bitcast.10, f32[8]{0:T(128)} %lam_ref.1, f32[1,64]{1,0:T(1,128)} %bitcast.11, f32[1,64]{1,0:T(1,128)} %bitcast.12, f32[1,128]{1,0:T(1,128)} %bitcast.13, ...), custom_call_target="tpu_custom_call" | custom-call | tf_op jit(solution)/shard_map/pallas_call | solution.py:341
  32.1 0.8 %copy.10 = bf16[1,128,2048]{2,1,0:T(8,128)(2,1)} copy(bf16[1,128,2048]{2,1,0:T(8,128)(2,1)S(1)} %bitcast.7) | data formatting | bytes 1048576

commit v3 on v2

--- a/solution.py
+++ b/solution.py
@@ -87,9 +87,10 @@
 
 
 def kernel(
-    sp, dp, q_ref, k_ref, v_ref, lam_ref, qg_ref, kg_ref, sg_ref, w_ref, out_ref,
+    sp, dp, q_ref, k_ref, v_ref, lam_in, qg_in, kg_in, sg_in, w_ref, out_ref,
     qb, kb, vb, kn, first, nsend, nbuf, wbuf,
     in_send, in_recv, back_send, back_recv, w_send, w_recv, p_send, p_recv, own_sem,
+    lam_ref, qg_ref, kg_ref, sg_ref, small_sem,
 ):
     me, d = lax.axis_index("sp"), lax.axis_index("dp")
     partner = d + 1 - 2 * lax.rem(d, 2)
@@ -201,6 +202,10 @@
             device_id=(i, d), device_id_type=MESH,
         )
 
+    small = [
+        pltpu.make_async_copy(src, dst, small_sem.at[n])
+        for n, (src, dst) in enumerate(((lam_in, lam_ref), (qg_in, qg_ref), (kg_in, kg_ref), (sg_in, sg_ref)))
+    ]
     for t in range(5):
         mine(t).start()
         for o in range(1, sp):
@@ -212,11 +217,15 @@
                         spread(c, (c + 1 + order) % 2).start()
             pair(0).start()
             own_weights().start()
+            for copy in small:
+                copy.start()
     if square:
         for h in range(2):
             gained(1 + h, h)
             spread(3, h).start()
 
+    for copy in small:
+        copy.wait()
     lane = lax.broadcasted_iota(jnp.int32, (width, width), 1) // HK
     ones = (lane == lax.broadcasted_iota(jnp.int32, (width, width), 0) // HK).astype(jnp.bfloat16)
     head_of = lax.broadcasted_iota(jnp.int32, (rows, width), 1) // HK
@@ -341,7 +350,7 @@
     out = pl.pallas_call(
         functools.partial(kernel, sp, dp),
         out_shape=pltpu.VMEM((rows, columns * dp), jnp.bfloat16),
-        in_specs=[hbm] * 3 + [pl.BlockSpec(memory_space=pltpu.SMEM)] + [vmem] * 3 + [hbm],
+        in_specs=[hbm] * 8,
         out_specs=vmem,
         scratch_shapes=[
             pltpu.VMEM((2, length, width), jnp.bfloat16),
@@ -354,6 +363,9 @@
             pltpu.VMEM((dp, depth, columns), jnp.bfloat16),
             dma((sp, 5)), dma((sp, 5)), dma((sp,)), dma((sp,)),
             dma((dp // 2, 2)), dma((dp // 2, 2)), dma((dp // 2,)), dma((dp // 2,)), dma,
+            pltpu.SMEM(lambdas.shape, jnp.float32),
+            pltpu.VMEM((1, HK), jnp.float32), pltpu.VMEM((1, HK), jnp.float32), pltpu.VMEM((1, HV), jnp.float32),
+            dma((4,)),
         ],
         compiler_params=pltpu.CompilerParams(collective_id=0, has_side_effects=True),
     )(

time: 33.1 us -> 32.3 us (0.976)
  Pallas kernels: 32.1 us -> 31.3 us
    pallas_call x1, Pallas kernels: 32.1 us -> 31.3 us  [fused(): pl.pallas_call(functools.partial(kernel, sp, dp), out_shape=pltpu.VMEM((r...]
where the time goes in v3:
time: 32.3 us; the launch traced here: 32.1 us
  Pallas kernels  31.3 us (97%)
  local copies, waits for them, and re-layouts  0.8 us (2%)
    pallas_call x1, Pallas kernels, fused(): pl.pallas_call(functools.partial(kernel, sp, dp), out_shape=pltpu.VMEM((r...  31.3 us
    unnamed x1, local copies, waits for them, and re-layouts  0.8 us

profile of v3, /device:TPU:0, one launch (start us, length us, event | category | flops | bytes accessed | tf_op | source)
XLA Modules:
  0.0 32.1 jit_solution(5687610637175810681)
XLA Ops:
  0.0 31.3 %shard_map.82 = bf16[128,2048]{1,0:T(8,128)(2,1)S(1)} custom-call(bf16[128,1024]{1,0:T(8,128)(2,1)} %bitcast.8, bf16[128,1024]{1,0:T(8,128)(2,1)} %bitcast.9, bf16[128,1024]{1,0:T(8,128)(2,1)} %bitcast.10, f32[8]{0:T(128)} %lam_in.1, f32[1,64]{1,0:T(1,128)} %bitcast.11, f32[1,64]{1,0:T(1,128)} %bitcast.12, f32[1,128]{1,0:T(1,128)} %bitcast.13, ...), custom_call_target="tpu_custom_call" | custom-call | tf_op jit(solution)/shard_map/pallas_call | solution.py:350
  31.4 0.8 %copy.10 = bf16[1,128,2048]{2,1,0:T(8,128)(2,1)} copy(bf16[1,128,2048]{2,1,0:T(8,128)(2,1)S(1)} %bitcast.7) | data formatting | bytes 1048576

commit v4 on v3

--- a/solution.py
+++ b/solution.py
@@ -81,15 +81,15 @@
 
 
 def fits(sp, dp, rows_shape, weight_shape):
-    if HEADS % sp or (HEADS // sp * HK) % 128 or dp % 2:
+    if sp != 4 or HEADS % sp or (HEADS // sp * HK) % 128 or dp % 2:
         return False
     return rows_shape[0] == 1 and rows_shape[1] % 128 == 0 and rows_shape[1] * sp <= 1024 and weight_shape[1] % 128 == 0
 
 
 def kernel(
     sp, dp, q_ref, k_ref, v_ref, lam_in, qg_in, kg_in, sg_in, w_ref, out_ref,
-    qb, kb, vb, kn, first, nsend, nbuf, wbuf,
-    in_send, in_recv, back_send, back_recv, w_send, w_recv, p_send, p_recv, own_sem,
+    qb, kb, vb, kn, qx, kx, vx, knx, nsend, nbuf, wbuf,
+    local_sem, in_send, in_recv, back_send, back_recv, w_send, w_recv, p_send, p_recv, own_sem,
     lam_ref, qg_ref, kg_ref, sg_ref, small_sem,
 ):
     me, d = lax.axis_index("sp"), lax.axis_index("dp")
@@ -119,46 +119,71 @@
     pl.semaphore_signal(barrier, inc=1, device_id=(me, partner), device_id_type=MESH)
     pl.semaphore_wait(barrier, sp - 1 + chips)
 
-    def span(i):
-        return pl.ds(pl.multiple_of(i * rows, rows), rows)
-
-    def pieces(target, source):
-        low = pl.ds(pl.multiple_of(target * width, 128), width)
-        high = pl.ds(pl.multiple_of(HEADS * HK + target * width, 128), width)
-        vals = pl.ds(pl.multiple_of(target * vwidth, 128), vwidth)
-        there = span(source)
-        return (
-            (k_ref.at[:, low], kb.at[0, there, :]),
-            (q_ref.at[:, low], qb.at[0, there, :]),
-            (v_ref.at[:, vals], vb.at[there, :]),
-            (k_ref.at[:, high], kb.at[1, there, :]),
-            (q_ref.at[:, high], qb.at[1, there, :]),
+    half_sp = sp // 2
+    lows, highs = range(half_sp), range(half_sp, sp)
+
+    def at(i):
+        return pl.ds(i * rows, rows)
+
+    def cols(pair_, m=0, count=1):
+        return pl.ds(m * HEADS * HK + pair_ * width, count * width)
+
+    def vcols(pair_, count=1):
+        return pl.ds(pair_ * vwidth, count * vwidth)
+
+    plan = {}
+    for z in range(sp):
+        for o in range(sp):
+            for m in range(2):
+                if o != z and (o in lows or z in highs):
+                    plan[z, o, "q", m] = q_ref.at[:, cols(o, m)], qb.at[m, at(z), :]
+                if o != z and (o in lows or z != 0):
+                    plan[z, o, "k", m] = k_ref.at[:, cols(o, m)], kb.at[m, at(z), :]
+            if o != z and (o in lows or z != 0):
+                plan[z, o, "v", 0] = v_ref.at[:, vcols(o)], vb.at[at(z), :]
+    for m in range(2):
+        plan[0, 1, "kx", m] = k_ref.at[:, cols(half_sp, m, half_sp)], kx.at[m, at(0), :]
+    plan[0, 1, "vx", 0] = v_ref.at[:, vcols(half_sp, half_sp)], vx.at[at(0), :]
+    for o in highs:
+        for m in range(2):
+            plan[1, o, "rk", m] = kx.at[m, at(0), cols(o - half_sp)], kb.at[m, at(0), :]
+        plan[1, o, "rv", 0] = vx.at[at(0), vcols(o - half_sp)], vb.at[at(0), :]
+    number = {key: n for n, key in enumerate(plan)}
+
+    def move(*key):
+        src, dst = plan[key]
+        n = number[key]
+        return pltpu.make_async_remote_copy(
+            src_ref=src, dst_ref=dst, send_sem=in_send.at[n], recv_sem=in_recv.at[n],
+            device_id=(key[1], d), device_id_type=MESH,
         )
 
-    def forward(o, t):
-        target = lax.rem(me + o, sp)
-        src, dst = pieces(target, me)[t]
-        return pltpu.make_async_remote_copy(
-            src_ref=src, dst_ref=dst, send_sem=in_send.at[o, t], recv_sem=in_recv.at[me, t],
-            device_id=(target, d), device_id_type=MESH,
-        )
-
-    def mine(t):
-        src, dst = pieces(me, me)[t]
-        return pltpu.make_async_copy(src, dst, in_recv.at[me, t])
-
-    def arrived(i, t):
-        @pl.when(i == me)
-        def _():
-            mine(t).wait()
-
-        @pl.when(i != me)
-        def _():
-            src, dst = pieces(me, i)[t]
-            pltpu.make_async_remote_copy(
-                src_ref=src, dst_ref=dst, send_sem=in_send.at[0, t], recv_sem=in_recv.at[i, t],
-                device_id=(me, d), device_id_type=MESH,
-            ).wait_recv()
+    def rows_in(z):
+        copies = []
+        for m in range(2):
+            copies.append((k_ref.at[:, cols(z, m)], kb.at[m, at(z), :]))
+            copies.append((q_ref.at[:, cols(z, m)], qb.at[m, at(z), :]))
+            if z in lows:
+                copies.append((k_ref.at[:, cols(half_sp, m, half_sp)], kx.at[m, at(z), :]))
+                copies.append((q_ref.at[:, cols(half_sp, m, half_sp)], qx.at[m]))
+        copies.append((v_ref.at[:, vcols(z)], vb.at[at(z), :]))
+        if z in lows:
+            copies.append((v_ref.at[:, vcols(half_sp, half_sp)], vx.at[at(z), :]))
+        return [pltpu.make_async_copy(src, dst, local_sem.at[n]) for n, (src, dst) in enumerate(copies)]
+
+    five = (("k", 0), ("q", 0), ("v", 0), ("k", 1), ("q", 1))
+    three = (("k", 0), ("v", 0), ("k", 1))
+
+    def outgoing(z):
+        if z == 0:
+            return [(0, 1, "kx", 0), (0, 1, "vx", 0), (0, 1, "kx", 1)] + [(0, 1) + f for f in five]
+        if z == 1:
+            return [(1, o) + f for f in three for o in highs] + [(1, 0) + f for f in five]
+        if z == 2:
+            return [(2, 0) + f for f in five] + [(2, 1) + f for f in five] + [(2, 3) + f for f in five]
+        return [(3, 0) + f for f in five] + [(3, 2) + f for f in five] + [(3, 1) + f for f in five]
+
+    relays = (("kx", "rk", 0), ("vx", "rv", 0), ("kx", "rk", 1))
 
     def rows_of(h):
         return pl.ds(h * half, half)
@@ -196,9 +221,9 @@
             device_id=(me, partner), device_id_type=MESH,
         )
 
-    def back(i):
+    def back(z, i):
         return pltpu.make_async_remote_copy(
-            src_ref=nsend.at[i], dst_ref=nbuf.at[me], send_sem=back_send.at[i], recv_sem=back_recv.at[me],
+            src_ref=nsend.at[i], dst_ref=nbuf.at[z], send_sem=back_send.at[i], recv_sem=back_recv.at[z],
             device_id=(i, d), device_id_type=MESH,
         )
 
@@ -206,26 +231,46 @@
         pltpu.make_async_copy(src, dst, small_sem.at[n])
         for n, (src, dst) in enumerate(((lam_in, lam_ref), (qg_in, qg_ref), (kg_in, kg_ref), (sg_in, sg_ref)))
     ]
-    for t in range(5):
-        mine(t).start()
-        for o in range(1, sp):
-            forward(o, t).start()
-        if t == 0:
-            for order in range(2):
-                for c in range(1, chips):
-                    if not (square and c == 3):
-                        spread(c, (c + 1 + order) % 2).start()
-            pair(0).start()
-            own_weights().start()
-            for copy in small:
+    for z in range(sp):
+        @pl.when(me == z)
+        def _(z=z):
+            for key in outgoing(z):
+                move(*key).start()
+
+    for order in range(2):
+        for c in range(1, chips):
+            if not (square and c == 3):
+                spread(c, (c + 1 + order) % 2).start()
+    pair(0).start()
+    for z in range(sp):
+        @pl.when(me == z)
+        def _(z=z):
+            for copy in rows_in(z):
                 copy.start()
-    if square:
-        for h in range(2):
-            gained(1 + h, h)
-            spread(3, h).start()
-
+    own_weights().start()
+    for copy in small:
+        copy.start()
     for copy in small:
         copy.wait()
+
+    def weights_first():
+        if square:
+            for h in range(2):
+                gained(1 + h, h)
+                spread(3, h).start()
+
+    def weights_next():
+        if square:
+            for h in range(2):
+                gained(1 + h, 1 - h)
+                pair(1 + h).start()
+
+    def weights_last():
+        for c in range(3 if square else 1, chips):
+            for h in range(2):
+                gained(c, h)
+            pair(c).start()
+
     lane = lax.broadcasted_iota(jnp.int32, (width, width), 1) // HK
     ones = (lane == lax.broadcasted_iota(jnp.int32, (width, width), 0) // HK).astype(jnp.bfloat16)
     head_of = lax.broadcasted_iota(jnp.int32, (rows, width), 1) // HK
@@ -244,67 +289,116 @@
         total += jnp.dot(lower, ones, preferred_element_type=jnp.float32)
         return (field * lax.rsqrt(total * (1.0 / HK) + epsilon) * gain).astype(jnp.bfloat16)
 
-    def attend_block(m, i):
-        base, keys = i * rows, (i + 1) * rows
-        kn[m, base:keys, :] = normed_rows(kb[m, base:keys, :], key_gain)
-        query = normed_rows(qb[m, base:keys, :], query_gain)
+    def attend(query, keys, vals, before):
+        query = normed_rows(query, query_gain)
         zero = jnp.zeros_like(query)
         stacked = jnp.concatenate([jnp.where(head_of == h, query, zero) for h in range(local)], axis=0)
         scores = lax.dot_general(
-            stacked, kn[m, :keys, :], (((1,), (1,)), ((), ())), preferred_element_type=jnp.float32
+            stacked, keys, (((1,), (1,)), ((), ())), preferred_element_type=jnp.float32
         ) * HK ** (-0.5)
-        last = jnp.where(visible, scores[:, base:], -jnp.inf)
-        scores = last if i == 0 else jnp.concatenate([scores[:, :base], last], axis=1)
+        last = jnp.where(visible, scores[:, before:], -jnp.inf)
+        scores = last if before == 0 else jnp.concatenate([scores[:, :before], last], axis=1)
         raised = jnp.exp(scores - jnp.max(scores, axis=1, keepdims=True))
         weights = (raised * (1.0 / jnp.sum(raised, axis=1, keepdims=True))).astype(jnp.bfloat16)
         return [
             jnp.dot(
-                weights[h * rows : (h + 1) * rows], vb[:keys, h * HV : (h + 1) * HV],
+                weights[h * rows : (h + 1) * rows], vals[:, h * HV : (h + 1) * HV],
                 preferred_element_type=jnp.float32,
             ).astype(jnp.bfloat16)
             for h in range(local)
         ]
 
-    for i in range(sp):
-        for t in range(3):
-            arrived(i, t)
-        for h, part in enumerate(attend_block(0, i)):
-            first[i * rows : (i + 1) * rows, h * HV : (h + 1) * HV] = part
-
-    if square:
-        for h in range(2):
-            gained(1 + h, 1 - h)
-            pair(1 + h).start()
-
-    for i in range(sp):
-        for t in range(3, 5):
-            arrived(i, t)
-        for h, part in enumerate(attend_block(1, i)):
-            before = first[i * rows : (i + 1) * rows, h * HV : (h + 1) * HV].astype(jnp.float32)
-            mixed = before - lam_ref[me * local + h] * part.astype(jnp.float32)
+    def mix(pair_, maps):
+        parts = []
+        for h in range(local):
+            mixed = maps[0][h].astype(jnp.float32) - lam_ref[pair_ * local + h] * maps[1][h].astype(jnp.float32)
             mean = jnp.mean(mixed * mixed, axis=1, keepdims=True)
-            nsend[i, :, h * HV : (h + 1) * HV] = (mixed * lax.rsqrt(mean + epsilon) * sub_gain).astype(jnp.bfloat16)
-
-        @pl.when(i == me)
-        def _():
-            nbuf[i] = nsend[i]
-
-        @pl.when(i != me)
-        def _():
-            back(i).start()
-
-    for c in range(3 if square else 1, chips):
-        for h in range(2):
-            gained(c, h)
-        pair(c).start()
-
-    for i in range(sp):
-        @pl.when(i != me)
-        def _():
-            pltpu.make_async_remote_copy(
-                src_ref=nsend.at[i], dst_ref=nbuf.at[i], send_sem=back_send.at[i], recv_sem=back_recv.at[i],
-                device_id=(i, d), device_id_type=MESH,
-            ).wait_recv()
+            parts.append((mixed * lax.rsqrt(mean + epsilon) * sub_gain).astype(jnp.bfloat16))
+        return jnp.concatenate(parts, axis=1)
+
+    def new_keys(m, i):
+        kn[m, i * rows : (i + 1) * rows, :] = normed_rows(kb[m, i * rows : (i + 1) * rows, :], key_gain)
+
+    def pair_map(m, i):
+        keys = (i + 1) * rows
+        return attend(qb[m, i * rows : keys, :], kn[m, :keys, :], vb[:keys, :], i * rows)
+
+    def near(z):
+        keys = (z + 1) * rows
+        for p in range(half_sp):
+            maps = []
+            for m in range(2):
+                for i in range(z + 1):
+                    knx[m, i * rows : (i + 1) * rows, :] = normed_rows(
+                        kx[m, i * rows : (i + 1) * rows, p * width : (p + 1) * width], key_gain
+                    )
+                maps.append(attend(
+                    qx[m, :, p * width : (p + 1) * width], knx[m, :keys, :],
+                    vx[:keys, p * vwidth : (p + 1) * vwidth], z * rows,
+                ))
+            nbuf[half_sp + p] = mix(half_sp + p, maps)
+
+    def give(z, i, maps):
+        if i == z:
+            nbuf[z] = mix(z, maps)
+        else:
+            nsend[i] = mix(z, maps)
+            back(z, i).start()
+
+    def below(z):
+        for copy in rows_in(z):
+            copy.wait()
+        if z == 1:
+            for held, sent, m in relays:
+                move(0, 1, held, m).wait_recv()
+                for o in highs:
+                    move(1, o, sent, m).start()
+        near(z)
+        weights_first()
+        for i in range(sp):
+            maps = []
+            for m in range(2):
+                if i != z:
+                    for f in five[3 * m : 3 + 2 * m]:
+                        move(i, z, *f).wait_recv()
+                new_keys(m, i)
+                maps.append(pair_map(m, i))
+            give(z, i, maps)
+            if i == half_sp:
+                weights_next()
+
+    def above(z):
+        for copy in rows_in(z):
+            copy.wait()
+        weights_first()
+        weights_next()
+        other = half_sp + sp - 1 - z
+        both = {i: [] for i in highs}
+        for m in range(2):
+            for f in five[3 * m : 3 + 2 * m]:
+                move(other, z, *f).wait_recv()
+                if f[0] != "q":
+                    move(1, z, *f).wait_recv()
+                    move(0 + 1, z, "r" + f[0], f[1]).wait_recv()
+            for i in range(sp):
+                new_keys(m, i)
+            for i in (other, z):
+                both[i].append(pair_map(m, i))
+        for i in (other, z):
+            give(z, i, both[i])
+
+    for z in range(sp):
+        @pl.when(me == z)
+        def _(z=z):
+            below(z) if z in lows else above(z)
+
+    weights_last()
+    for z in range(sp):
+        @pl.when(me == z)
+        def _(z=z):
+            for o in range(sp):
+                if o != z and (o in lows or z in highs):
+                    back(o, z).wait_recv()
 
     normed = jnp.concatenate([nbuf[j] for j in range(sp)], axis=1)
 
@@ -324,18 +418,23 @@
         ).wait_recv()
         project(at, wbuf[at])
 
-    for o in range(1, sp):
-        for t in range(5):
-            forward(o, t).wait_send()
+    for z in range(sp):
+        @pl.when(me == z)
+        def _(z=z):
+            for key in outgoing(z):
+                move(*key).wait_send()
+            if z == 1:
+                for _, sent, m in relays:
+                    for o in highs:
+                        move(1, o, sent, m).wait_send()
+            for i in range(sp):
+                if i != z and (z in lows or i in highs):
+                    back(z, i).wait_send()
     for c in range(chips):
         pair(c).wait_send()
         if c:
             for h in range(2):
                 spread(c, h).wait_send()
-    for i in range(sp):
-        @pl.when(i != me)
-        def _():
-            back(i).wait_send()
 
 
 def fused(sp, dp, query_rows, key_rows, value_rows, lambdas, query_gain, key_gain, sub_gain, out_weight):
@@ -357,11 +456,14 @@
             pltpu.VMEM((2, length, width), jnp.bfloat16),
             pltpu.VMEM((length, vwidth), jnp.bfloat16),
             pltpu.VMEM((2, length, width), jnp.bfloat16),
-            pltpu.VMEM((length, vwidth), jnp.bfloat16),
+            pltpu.VMEM((2, rows, sp // 2 * width), jnp.bfloat16),
+            pltpu.VMEM((2, sp // 2 * rows, sp // 2 * width), jnp.bfloat16),
+            pltpu.VMEM((sp // 2 * rows, sp // 2 * vwidth), jnp.bfloat16),
+            pltpu.VMEM((2, sp // 2 * rows, width), jnp.bfloat16),
             pltpu.VMEM((sp, rows, vwidth), jnp.bfloat16),
             pltpu.VMEM((sp, rows, vwidth), jnp.bfloat16),
             pltpu.VMEM((dp, depth, columns), jnp.bfloat16),
-            dma((sp, 5)), dma((sp, 5)), dma((sp,)), dma((sp,)),
+            dma((10,)), dma((5 * sp * sp,)), dma((5 * sp * sp,)), dma((sp,)), dma((sp,)),
             dma((dp // 2, 2)), dma((dp // 2, 2)), dma((dp // 2,)), dma((dp // 2,)), dma,
             pltpu.SMEM(lambdas.shape, jnp.float32),
             pltpu.VMEM((1, HK), jnp.float32), pltpu.VMEM((1, HK), jnp.float32), pltpu.VMEM((1, HV), jnp.float32),

time: 32.3 us -> 31.2 us (0.966)
  the two profiles are of different devices: /device:TPU:0 before, /device:TPU:24 now
where the time goes in v4:
time: 31.2 us; the launch traced here: 31 us
  Pallas kernels  30.2 us (97%)
  local copies, waits for them, and re-layouts  0.8 us (3%)
    pallas_call x1, Pallas kernels, fused(): pl.pallas_call(functools.partial(kernel, sp, dp), out_shape=pltpu.VMEM((r...  30.2 us
    unnamed x1, local copies, waits for them, and re-layouts  0.8 us

profile of v4, /device:TPU:24, one launch (start us, length us, event | category | flops | bytes accessed | tf_op | source)
XLA Modules:
  0.0 31.0 jit_solution(2764754432188713161)
XLA Ops:
  0.0 30.2 %shard_map.82 = bf16[128,2048]{1,0:T(8,128)(2,1)S(1)} custom-call(bf16[128,1024]{1,0:T(8,128)(2,1)} %bitcast.8, bf16[128,1024]{1,0:T(8,128)(2,1)} %bitcast.9, bf16[128,1024]{1,0:T(8,128)(2,1)} %bitcast.10, f32[8]{0:T(128)} %lam_in.1, f32[1,64]{1,0:T(1,128)} %bitcast.11, f32[1,64]{1,0:T(1,128)} %bitcast.12, f32[1,128]{1,0:T(1,128)} %bitcast.13, ...), custom_call_target="tpu_custom_call" | custom-call | tf_op jit(solution)/shard_map/pallas_call | solution.py:449
  30.2 0.8 %copy.10 = bf16[1,128,2048]{2,1,0:T(8,128)(2,1)} copy(bf16[1,128,2048]{2,1,0:T(8,128)(2,1)S(1)} %bitcast.7) | data formatting | bytes 1048576

commit v5 on v4

--- a/solution.py
+++ b/solution.py
@@ -90,7 +90,7 @@
     sp, dp, q_ref, k_ref, v_ref, lam_in, qg_in, kg_in, sg_in, w_ref, out_ref,
     qb, kb, vb, kn, qx, kx, vx, knx, nsend, nbuf, wbuf,
     local_sem, in_send, in_recv, back_send, back_recv, w_send, w_recv, p_send, p_recv, own_sem,
-    lam_ref, qg_ref, kg_ref, sg_ref, small_sem,
+    lam_ref, qg_ref, kg_ref, sg_ref, small_sem, acc,
 ):
     me, d = lax.axis_index("sp"), lax.axis_index("dp")
     partner = d + 1 - 2 * lax.rem(d, 2)
@@ -117,7 +117,6 @@
     for c in range(1, chips):
         pl.semaphore_signal(barrier, inc=1, device_id=(me, fellow(c)), device_id_type=MESH)
     pl.semaphore_signal(barrier, inc=1, device_id=(me, partner), device_id_type=MESH)
-    pl.semaphore_wait(barrier, sp - 1 + chips)
 
     half_sp = sp // 2
     lows, highs = range(half_sp), range(half_sp, sp)
@@ -181,7 +180,7 @@
             return [(1, o) + f for f in three for o in highs] + [(1, 0) + f for f in five]
         if z == 2:
             return [(2, 0) + f for f in five] + [(2, 1) + f for f in five] + [(2, 3) + f for f in five]
-        return [(3, 0) + f for f in five] + [(3, 2) + f for f in five] + [(3, 1) + f for f in five]
+        return [(3, 0) + f for f in five] + [(3, 1) + f for f in five] + [(3, 2) + f for f in five]
 
     relays = (("kx", "rk", 0), ("vx", "rv", 0), ("kx", "rk", 1))
 
@@ -234,6 +233,16 @@
     for z in range(sp):
         @pl.when(me == z)
         def _(z=z):
+            for copy in rows_in(z):
+                copy.start()
+    own_weights().start()
+    for copy in small:
+        copy.start()
+    pl.semaphore_wait(barrier, sp - 1 + chips)
+
+    for z in range(sp):
+        @pl.when(me == z)
+        def _(z=z):
             for key in outgoing(z):
                 move(*key).start()
 
@@ -242,14 +251,6 @@
             if not (square and c == 3):
                 spread(c, (c + 1 + order) % 2).start()
     pair(0).start()
-    for z in range(sp):
-        @pl.when(me == z)
-        def _(z=z):
-            for copy in rows_in(z):
-                copy.start()
-    own_weights().start()
-    for copy in small:
-        copy.start()
     for copy in small:
         copy.wait()
 
@@ -353,8 +354,8 @@
                 move(0, 1, held, m).wait_recv()
                 for o in highs:
                     move(1, o, sent, m).start()
+        weights_first()
         near(z)
-        weights_first()
         for i in range(sp):
             maps = []
             for m in range(2):
@@ -392,31 +393,40 @@
         def _(z=z):
             below(z) if z in lows else above(z)
 
+    def gather_back(owners):
+        for z in range(sp):
+            @pl.when(me == z)
+            def _(z=z):
+                for o in owners:
+                    if o != z and (o in lows or z in highs):
+                        back(o, z).wait_recv()
+
+    def project(shard, owners, first):
+        normed = jnp.concatenate([nbuf[j] for j in owners], axis=1)
+        weight = wbuf[shard, owners[0] * vwidth : (owners[-1] + 1) * vwidth, :]
+        here = pl.ds(pl.multiple_of(shard * columns, 128), columns)
+        total = jnp.dot(normed, weight, preferred_element_type=jnp.float32)
+        if first:
+            acc[:, here] = total
+        else:
+            out_ref[:, here] = (acc[:, here] + total).astype(jnp.bfloat16)
+
     weights_last()
-    for z in range(sp):
-        @pl.when(me == z)
-        def _(z=z):
-            for o in range(sp):
-                if o != z and (o in lows or z in highs):
-                    back(o, z).wait_recv()
-
-    normed = jnp.concatenate([nbuf[j] for j in range(sp)], axis=1)
-
-    def project(shard, weight):
-        out_ref[:, pl.ds(pl.multiple_of(shard * columns, 128), columns)] = jnp.dot(
-            normed, weight, preferred_element_type=jnp.float32
-        ).astype(jnp.bfloat16)
-
+    gather_back(highs)
     own_weights().wait()
     for c in range(chips):
-        project(shard_of(d, c), wbuf[shard_of(d, c)])
+        project(shard_of(d, c), highs, True)
     for c in range(chips):
-        at = shard_of(partner, c)
+        at_ = shard_of(partner, c)
         pltpu.make_async_remote_copy(
-            src_ref=wbuf.at[at], dst_ref=wbuf.at[at], send_sem=p_send.at[c], recv_sem=p_recv.at[c],
+            src_ref=wbuf.at[at_], dst_ref=wbuf.at[at_], send_sem=p_send.at[c], recv_sem=p_recv.at[c],
             device_id=(me, partner), device_id_type=MESH,
         ).wait_recv()
-        project(at, wbuf[at])
+        project(at_, highs, True)
+    gather_back(lows)
+    for c in range(chips):
+        project(shard_of(d, c), lows, False)
+        project(shard_of(partner, c), lows, False)
 
     for z in range(sp):
         @pl.when(me == z)
@@ -468,6 +478,7 @@
             pltpu.SMEM(lambdas.shape, jnp.float32),
             pltpu.VMEM((1, HK), jnp.float32), pltpu.VMEM((1, HK), jnp.float32), pltpu.VMEM((1, HV), jnp.float32),
             dma((4,)),
+            pltpu.VMEM((rows, columns * dp), jnp.float32),
         ],
         compiler_params=pltpu.CompilerParams(collective_id=0, has_side_effects=True),
     )(

time: 31.2 us -> 29.9 us (0.958)
  Pallas kernels: 30.2 us -> 29 us
    pallas_call x1, Pallas kernels: 30.2 us -> 29 us  [fused(): pl.pallas_call(functools.partial(kernel, sp, dp), out_shape=pltpu.VMEM((r...]
where the time goes in v5:
time: 29.9 us; the launch traced here: 29.8 us
  Pallas kernels  29 us (97%)
  local copies, waits for them, and re-layouts  0.8 us (3%)
    pallas_call x1, Pallas kernels, fused(): pl.pallas_call(functools.partial(kernel, sp, dp), out_shape=pltpu.VMEM((r...  29 us
    unnamed x1, local copies, waits for them, and re-layouts  0.8 us

profile of v5, /device:TPU:24, one launch (start us, length us, event | category | flops | bytes accessed | tf_op | source)
XLA Modules:
  0.0 29.8 jit_solution(6421864550887947415)
XLA Ops:
  0.0 29.0 %shard_map.82 = bf16[128,2048]{1,0:T(8,128)(2,1)S(1)} custom-call(bf16[128,1024]{1,0:T(8,128)(2,1)} %bitcast.8, bf16[128,1024]{1,0:T(8,128)(2,1)} %bitcast.9, bf16[128,1024]{1,0:T(8,128)(2,1)} %bitcast.10, f32[8]{0:T(128)} %lam_in.1, f32[1,64]{1,0:T(1,128)} %bitcast.11, f32[1,64]{1,0:T(1,128)} %bitcast.12, f32[1,128]{1,0:T(1,128)} %bitcast.13, ...), custom_call_target="tpu_custom_call" | custom-call | tf_op jit(solution)/shard_map/pallas_call | solution.py:459
  29.0 0.8 %copy.10 = bf16[1,128,2048]{2,1,0:T(8,128)(2,1)} copy(bf16[1,128,2048]{2,1,0:T(8,128)(2,1)S(1)} %bitcast.7) | data formatting | bytes 1048576
